TPU v7x, 32 devices: a whole 2x2x4 slice. The times are simulated.
32 devices in a mesh: grp: 2 (over y), sp: 8 (over z, core), tp: 2 (over x).
Axes of the slice: x: 2, y: 2, z: 4, core: 2. Of those that a mesh axis runs over, the one named last changes fastest.
Arguments:
- query_plain: bfloat16 [2560, 1024], P(('grp', 'sp'), 'tp'), parts along dimension 0, may hold values from -6 to 6
- query_turn: bfloat16 [2560, 512], P(('grp', 'sp'), 'tp'), parts along dimension 0, may hold values from -40 to 40, as said below
- latent: bfloat16 [2560, 512], P(('grp', 'sp')), parts along dimension 0, may hold values from -6 to 6
- key_turn: bfloat16 [2560, 64], P(('grp', 'sp')), parts along dimension 0, may hold values from -40 to 40, as said below
- latent_norm_scale: bfloat16 [512], replicated, may hold values from 0.099609375 to 1.8984375
- plain_key_matrix: bfloat16 [512, 1024], P(None, 'tp'), may hold values from -0.25 to 0.25
- value_matrix: bfloat16 [512, 1024], P(None, 'tp'), may hold values from -0.25 to 0.25
- residual: bfloat16 [2560, 2048], P(('grp', 'sp', 'tp')), parts along dimension 0, may hold values from -6 to 6
- out_weight: bfloat16 [1024, 2048], replicated, may hold values from -6 to 6
- ffn_gain: bfloat16 [2048], replicated, may hold values from 0.099609375 to 1.8984375
- gate_weight: bfloat16 [8, 2048, 1024], P('sp', None, 'tp'), may hold values from -1 to 1
- up_weight: bfloat16 [8, 2048, 1024], P('sp', None, 'tp'), may hold values from -1 to 1
- down_weight: bfloat16 [8, 1024, 2048], P('sp', 'tp'), may hold values from -0.0625 to 0.0625
- routes: int32 [2560, 4], P(('grp', 'sp', 'tp')), parts along dimension 0, may hold values from 0 to 7, all different within a row; in each aligned block of 80 rows (0 to 79, 80 to 159, ...) at most 60 rows name the same one
- route_weights: float32 [2560, 4], P(('grp', 'sp', 'tp')), parts along dimension 0, may hold values from 0.1 to 0.6
Outputs:
- mixed: bfloat16 [2560, 2048], P(('grp', 'sp', 'tp')), parts along dimension 0
There are 2 independent parts, one for each index of `grp`. A program takes and returns all parts, laid end to end along the dimension named above; an argument that names none is the same for every part. Nothing has to cross between parts.
Inputs may be any that keep to these rules, and one draw needn't show every extreme that they name: `query_turn`: in the hidden draw some rows are large. `key_turn`: in the hidden draw some rows are large. `routes`: each row names 4 different experts. In each aligned block of 80 rows (the rows of one device) no expert is named more than 60 times, a bound that some block reaches.
All inputs are finite; a program needn't handle non-finite values.
Results may differ from a plain program's by a relative error of at most 0.015.
Values may be sent and summed in bfloat16 or wider, within the bound.
A program may use at most 128 MiB of HBM per device.

v0:
```python
import jax
import jax.numpy as jnp
from jax import lax
from jax.sharding import PartitionSpec as P

PLAIN_HEAD_WIDTH = 128
QK_ROPE = 64
VALUE_WIDTH = 128
GRID_W = 64
theta = 10000.0
eps = 1e-06
limit = 7.0
slope = 1.702


def turn(vector, row_shift, col_shift):
    width = vector.shape[-1]
    count = width // 4
    half = width // 2
    freqs = theta ** (-jnp.arange(count, dtype=jnp.float32) / count)
    extra = (1,) * (vector.ndim - 2)
    pieces = []
    for portion, shift in ((vector[..., :half], row_shift), (vector[..., half:], col_shift)):
        angle = (shift.astype(jnp.float32)[:, None] * freqs[None, :]).reshape(
            (shift.shape[0],) + extra + (count,)
        )
        lower = portion[..., :count]
        upper = portion[..., count:]
        pieces.append(
            jnp.concatenate(
                [
                    lower * jnp.cos(angle) - upper * jnp.sin(angle),
                    lower * jnp.sin(angle) + upper * jnp.cos(angle),
                ],
                axis=-1,
            )
        )
    return jnp.concatenate(pieces, axis=-1)


def norm_scale(values, gain):
    wide = values.astype(jnp.float32)
    return (
        wide
        * lax.rsqrt(jnp.mean(wide * wide, axis=-1, keepdims=True) + eps)
        * gain.astype(jnp.float32)
    )


def expert_active(rows, gate_w, up_w):
    gate_pre = jnp.minimum(jnp.dot(rows, gate_w, preferred_element_type=jnp.float32), limit)
    up_pre = jnp.clip(jnp.dot(rows, up_w, preferred_element_type=jnp.float32), -limit, limit)
    return ((up_pre + 1.0) * gate_pre * jax.nn.sigmoid(slope * gate_pre)).astype(jnp.bfloat16)


def expert_whole(rows, gate_w, up_w, down_w, groups):
    active = expert_active(rows, gate_w, up_w)
    piece = down_w.shape[0] // groups
    total = jnp.zeros((rows.shape[0], down_w.shape[1]), jnp.float32)
    for index in range(groups):
        product = jnp.dot(
            active[:, index * piece : (index + 1) * piece],
            down_w[index * piece : (index + 1) * piece],
            preferred_element_type=jnp.float32,
        )
        total = total + product.astype(jnp.bfloat16).astype(jnp.float32)
    return total.astype(jnp.bfloat16)


def on_device(
    query_plain,
    query_turn,
    latent,
    key_turn,
    latent_norm_scale,
    plain_key_matrix,
    value_matrix,
    residual,
    out_weight,
    ffn_gain,
    gate_weight,
    up_weight,
    down_weight,
    routes,
    route_weights,
):
    tok_dev = latent.shape[0]
    heads_dev = query_plain.shape[1] // PLAIN_HEAD_WIDTH
    model_width = residual.shape[1]
    place = lax.axis_index("sp") * tok_dev + jnp.arange(tok_dev, dtype=jnp.int32)
    grid_row = place // GRID_W
    grid_col = place % GRID_W
    normed_latent = norm_scale(latent, latent_norm_scale).astype(jnp.bfloat16)
    key_plain = jnp.dot(normed_latent, plain_key_matrix, preferred_element_type=jnp.float32).astype(
        jnp.bfloat16
    )
    values = jnp.dot(normed_latent, value_matrix, preferred_element_type=jnp.float32).astype(
        jnp.bfloat16
    )
    key_rot = turn(key_turn.astype(jnp.float32), grid_row, grid_col).astype(jnp.bfloat16)
    key_pairs = key_rot.reshape(tok_dev // 2, 2 * QK_ROPE)
    query_rot = turn(
        query_turn.astype(jnp.float32).reshape(tok_dev, heads_dev, QK_ROPE), grid_row, grid_col
    ).astype(jnp.bfloat16)
    plain_query = query_plain.reshape(tok_dev, heads_dev, PLAIN_HEAD_WIDTH)
    scale = (PLAIN_HEAD_WIDTH + QK_ROPE) ** (-0.5)
    most = jnp.full((heads_dev, tok_dev), -jnp.inf, jnp.float32)
    total = jnp.zeros((heads_dev, tok_dev), jnp.float32)
    summed = jnp.zeros((heads_dev, tok_dev, VALUE_WIDTH), jnp.float32)
    piece_keys = lax.all_gather(key_plain, "sp", axis=0, tiled=True)
    piece_values = lax.all_gather(values, "sp", axis=0, tiled=True)
    piece_pairs = lax.all_gather(key_pairs, "sp", axis=0, tiled=True)
    count = piece_keys.shape[0]
    piece_rot = piece_pairs.reshape(count, QK_ROPE)
    new_most = []
    new_total = []
    new_summed = []
    for head in range(heads_dev):
        head_keys = piece_keys[:, head * PLAIN_HEAD_WIDTH : (head + 1) * PLAIN_HEAD_WIDTH]
        head_values = piece_values[:, head * VALUE_WIDTH : (head + 1) * VALUE_WIDTH]
        scores = (
            jnp.einsum(
                "qd,kd->qk", plain_query[:, head], head_keys, preferred_element_type=jnp.float32
            )
            + jnp.einsum(
                "qd,kd->qk", query_rot[:, head], piece_rot, preferred_element_type=jnp.float32
            )
        ) * scale
        peak = jnp.max(scores, axis=1)
        factor = jnp.exp(most[head] - peak)
        weights = jnp.exp(scores - peak[:, None])
        new_total.append(total[head] * factor + jnp.sum(weights, axis=1))
        new_summed.append(
            summed[head] * factor[:, None]
            + jnp.dot(weights.astype(jnp.bfloat16), head_values, preferred_element_type=jnp.float32)
        )
        new_most.append(peak)
    total = jnp.stack(new_total)
    summed = jnp.stack(new_summed)
    attended = jnp.transpose((summed / total[..., None]).astype(jnp.bfloat16), (1, 0, 2)).reshape(
        tok_dev, heads_dev * VALUE_WIDTH
    )
    rows_dev = residual.shape[0]
    own_rows = lax.dynamic_slice_in_dim(
        out_weight, lax.axis_index("tp") * heads_dev * VALUE_WIDTH, heads_dev * VALUE_WIDTH, 0
    )
    projected = lax.psum_scatter(
        jnp.dot(attended, own_rows, preferred_element_type=jnp.float32).astype(jnp.bfloat16),
        "tp",
        scatter_dimension=0,
        tiled=True,
    ).astype(jnp.float32)
    hidden = (residual.astype(jnp.float32) + projected).astype(jnp.bfloat16)
    normed = norm_scale(hidden, ffn_gain).astype(jnp.bfloat16)
    top_count = routes.shape[1]
    experts_all = lax.axis_size("sp") * gate_weight.shape[0]
    capacity = min(rows_dev, max(2, rows_dev * top_count * 3 // (2 * experts_all)))
    flat_routes = routes.reshape(rows_dev * top_count)
    marks = (flat_routes[:, None] == jnp.arange(experts_all, dtype=jnp.int32)[None, :]).astype(
        jnp.int32
    )
    earlier = jnp.cumsum(marks, axis=0, dtype=jnp.int32) - marks
    slots = jnp.sum(earlier * marks, axis=1, dtype=jnp.int32)
    target = flat_routes * capacity + slots
    chosen = (
        target.reshape(rows_dev, top_count)[None, :, :]
        == jnp.arange(experts_all * capacity, dtype=jnp.int32)[:, None, None]
    )
    dispatch_table = jnp.sum(chosen.astype(jnp.bfloat16), axis=2)
    outgoing = jnp.dot(dispatch_table, normed, preferred_element_type=jnp.float32).astype(
        jnp.bfloat16
    )
    outgoing = outgoing.reshape(experts_all, capacity, model_width)
    gate_w = gate_weight[0]
    up_w = up_weight[0]
    down_w = down_weight[0]
    group = lax.axis_size("tp")
    gate_full, up_full, down_full = (
        lax.all_gather(gate_w, "tp", axis=1, tiled=True),
        lax.all_gather(up_w, "tp", axis=1, tiled=True),
        lax.all_gather(down_w, "tp", axis=0, tiled=True),
    )
    arrived = lax.all_to_all(outgoing, "sp", split_axis=0, concat_axis=0, tiled=True)
    result_rows = expert_whole(
        arrived.reshape(experts_all * capacity, model_width), gate_full, up_full, down_full, group
    )
    returned = lax.all_to_all(
        result_rows.reshape(experts_all, capacity, model_width),
        "sp",
        split_axis=0,
        concat_axis=0,
        tiled=True,
    )
    picked = returned.reshape(experts_all * capacity, model_width)[target]
    picked = picked.reshape(rows_dev, top_count, model_width).astype(jnp.float32)
    return (hidden.astype(jnp.float32) + jnp.sum(route_weights[..., None] * picked, axis=1)).astype(
        jnp.bfloat16
    )


def solution(mesh):
    placed = (
        P(("grp", "sp"), "tp"),
        P(("grp", "sp"), "tp"),
        P(("grp", "sp"), None),
        P(("grp", "sp"), None),
        P(),
        P(None, "tp"),
        P(None, "tp"),
        P(("grp", "sp", "tp"), None),
        P(),
        P(),
        P("sp", None, "tp"),
        P("sp", None, "tp"),
        P("sp", "tp", None),
        P(("grp", "sp", "tp"), None),
        P(("grp", "sp", "tp"), None),
    )
    return jax.shard_map(
        on_device,
        mesh=mesh,
        in_specs=placed,
        out_specs=P(("grp", "sp", "tp"), None),
        check_vma=False,
    )
```

profile of v0, /device:TPU:0, one launch (start us, length us, event | category | flops | bytes accessed | tf_op | source)
XLA Modules:
  0.0 335.4 jit_solution(11522728959038800007)
XLA Ops:
  8.4 1.9 convolution_convert_fusion.5
  10.3 2.1 convolution_convert_fusion.4
  13.1 16.3 %all_gather.19 = bf16[640,128]{1,0:T(8,128)(2,1)S(1)} all-gather(bf16[80,128]{1,0:T(8,128)(2,1)S(1)} %convert_element_type.125), channel_id=1, replica_groups=mesh['grp'=2,'sp'=8,'tp'=2] {'sp'}, dimensions={0}, use_global_device_ids=true | all-gather | bytes 184320 | tf_op jit(solution)/shard_map/all_gather | solution.py:112
  30.0 7.3 %all-gather.9.cloned.1.call-done = bf16[1280,512]{1,0:T(8,128)(2,1)} async-done(((bf16[160,512]{1,0:T(8,128)(2,1)}), bf16[1280,512]{1,0:T(8,128)(2,1)}) %all-gather.9.cloned.1.call-update) | async-done | bytes 1310736 | tf_op jit(solution)/shard_map/all_gather | solution.py:110
  43.1 18.7 %all-gather.11.cloned.1.call-done = bf16[1280,512]{1,0:T(8,128)(2,1)} async-done(((bf16[160,512]{1,0:T(8,128)(2,1)}), bf16[1280,512]{1,0:T(8,128)(2,1)}) %all-gather.11.cloned.1.call-update) | async-done | bytes 1310736 | tf_op jit(solution)/shard_map/all_gather | solution.py:111
  65.3 3.0 convolution_convert_fusion.3
  71.4 12.7 %reduce-scatter.2.cloned.1.call-done = bf16[80,2048]{1,0:T(8,128)(2,1)} async-done(((bf16[160,2048]{1,0:T(8,128)(2,1)}), bf16[80,2048]{1,0:T(8,128)(2,1)}) %reduce-scatter.2.cloned.1.call-update) | async-done | bytes 327696 | tf_op jit(solution)/shard_map/reduce_scatter | solution.py:147
  85.3 1.7 convolution_convert_fusion.2
  87.0 1.6 reshape.371
  88.6 4.6 %all-to-all-start = ((bf16[8,60,2048]{2,1,0:T(8,128)(2,1)}), bf16[8,60,2048]{2,1,0:T(8,128)(2,1)S(1)}, u32[]{:S(2)}, u32[]{:S(2)}) async-start(bf16[8,60,2048]{2,1,0:T(8,128)(2,1)} %reshape.371), calls=%async_computation.1 | async-start | bytes 4194304 | tf_op jit(solution)/shard_map/all_to_all | solution.py:183
  93.8 48.5 %all-to-all-done = bf16[8,60,2048]{2,1,0:T(8,128)(2,1)S(1)} async-done(((bf16[8,60,2048]{2,1,0:T(8,128)(2,1)}), bf16[8,60,2048]{2,1,0:T(8,128)(2,1)S(1)}, u32[]{:S(2)}, u32[]{:S(2)}) %all-to-all-start) | async-done | bytes 1966112 | tf_op jit(solution)/shard_map/all_to_all | solution.py:183
  142.2 1.5 reshape.372
  143.7 6.4 %fusion = f32[480,1024]{1,0:T(8,128)} fusion(bf16[480,2048]{1,0:T(8,128)(2,1)} %reshape.372, bf16[1,2048,1024]{2,1,0:T(8,128)(2,1)} %all-gather.15.cloned.1.call-done), kind=kOutput, calls=%fused_computation.1 | convolution fusion | flops 2013265920 | bytes 8126464 | tf_op jit(solution)/shard_map/dot_general | solution.py:51
  150.1 50.3 %all-gather.13.cloned.1.call-done = bf16[1,2048,1024]{2,1,0:T(8,128)(2,1)} async-done(((bf16[1,2048,512]{2,1,0:T(8,128)(2,1)}), bf16[1,2048,1024]{2,1,0:T(8,128)(2,1)}) %all-gather.13.cloned.1.call-update) | async-done | bytes 4194320 | tf_op jit(solution)/shard_map/all_gather | solution.py:180
  200.4 6.5 %multiply_convert_fusion = bf16[480,1024]{1,0:T(8,128)(2,1)} fusion(f32[480,1024]{1,0:T(8,128)} %fusion, bf16[480,2048]{1,0:T(8,128)(2,1)S(1)} %copy-done.5, bf16[1,2048,1024]{2,1,0:T(8,128)(2,1)} %all-gather.13.cloned.1.call-done), kind=kOutput, calls=%fused_computation.26 | convolution fusion | flops 2018181120 | bytes 9109504 | tf_op jit(solution)/shard_map/dot_general | solution.py:52
  206.9 51.7 %all-gather.17.cloned.1.call-done = bf16[1,1024,2048]{2,1,0:T(8,128)(2,1)} async-done(((bf16[1,512,2048]{2,1,0:T(8,128)(2,1)}), bf16[1,1024,2048]{2,1,0:T(8,128)(2,1)}) %all-gather.17.cloned.1.call-update) | async-done | bytes 4194320 | tf_op jit(solution)/shard_map/all_gather | solution.py:181
  258.6 3.1 convolution_convert_fusion
  263.0 1.5 reshape.373
  264.5 4.7 %all-to-all-start.1 = ((bf16[8,60,2048]{2,1,0:T(8,128)(2,1)}), bf16[8,60,2048]{2,1,0:T(8,128)(2,1)}, u32[]{:S(2)}, u32[]{:S(2)}) async-start(bf16[8,60,2048]{2,1,0:T(8,128)(2,1)} %reshape.373), calls=%async_computation.2 | async-start | bytes 4194304 | tf_op jit(solution)/shard_map/all_to_all | solution.py:187
  269.5 48.9 %all-to-all-done.1 = bf16[8,60,2048]{2,1,0:T(8,128)(2,1)} async-done(((bf16[8,60,2048]{2,1,0:T(8,128)(2,1)}), bf16[8,60,2048]{2,1,0:T(8,128)(2,1)}, u32[]{:S(2)}, u32[]{:S(2)}) %all-to-all-start.1) | async-done | bytes 1966112 | tf_op jit(solution)/shard_map/all_to_all | solution.py:187
  318.4 1.7 reshape.374
  320.1 3.0 gather_fusion
  323.2 2.6 reshape.378
  325.8 1.9 multiply_reduce_fusion
  (105 shorter events, 19.4 us)
Async XLA Ops:
  6.5 1.9 copy-start
  6.5 6.0 %copy-start.10 = (bf16[160,64]{0,1:T(8,128)(2,1)S(1)}, bf16[160,64]{0,1:T(8,128)(2,1)}, u32[]{:S(2)}) copy-start(bf16[160,64]{0,1:T(8,128)(2,1)} %param.18) | copy-start | bytes 61444
  6.5 6.0 %copy-start.9 = (bf16[160,256]{1,0:T(8,128)(2,1)S(1)}, bf16[160,256]{1,0:T(8,128)(2,1)}, u32[]{:S(2)}) copy-start(bf16[160,256]{1,0:T(8,128)(2,1)} %param.16) | copy-start | bytes 245764
  6.5 23.0 %copy-start.8 = (bf16[160,512]{1,0:T(8,128)(2,1)S(1)}, bf16[160,512]{1,0:T(8,128)(2,1)}, u32[]{:S(2)}) copy-start(bf16[160,512]{1,0:T(8,128)(2,1)} %param.15) | copy-start | bytes 491524
  6.5 30.7 %all-gather.9.cloned.1.call-start = ((), (), s32[]{:S(2)}) async-start(), calls=%async_computation.3 | async-start | bytes 1474560 | tf_op jit(solution)/shard_map/all_gather | solution.py:110
  10.3 51.6 %all-gather.11.cloned.1.call-start = ((), (), s32[]{:S(2)}) async-start(), calls=%async_computation.4 | async-start | bytes 1474560 | tf_op jit(solution)/shard_map/all_gather | solution.py:111
  12.4 71.7 %reduce-scatter.2.cloned.1.call-start = ((), (), s32[]{:S(2)}) async-start(), calls=%async_computation.5 | async-start | bytes 983040 | tf_op jit(solution)/shard_map/reduce_scatter | solution.py:147
  37.2 1.8 copy-start.6
  41.8 0.9 copy-start.1
  61.8 2.8 copy-start.7
  61.8 3.1 copy-start.2
  68.3 1.2 copy-start.12
  68.3 2.9 copy-start.11
  68.4 15.7 %copy-start.3 = (bf16[80,2048]{1,0:T(8,128)(2,1)S(1)}, bf16[80,2048]{1,0:T(8,128)(2,1)}, u32[]{:S(2)}) copy-start(bf16[80,2048]{1,0:T(8,128)(2,1)} %param.22) | copy-start | bytes 983044
  68.4 75.3 %all-gather.15.cloned.1.call-start = ((), (), s32[]{:S(2)}) async-start(), calls=%async_computation.7 | async-start | bytes 6291456 | tf_op jit(solution)/shard_map/all_gather | solution.py:179
  68.9 131.5 %all-gather.13.cloned.1.call-start = ((), (), s32[]{:S(2)}) async-start(), calls=%async_computation.6 | async-start | bytes 6291456 | tf_op jit(solution)/shard_map/all_gather | solution.py:180
  88.6 53.6 %all-to-all-start = ((bf16[8,60,2048]{2,1,0:T(8,128)(2,1)}), bf16[8,60,2048]{2,1,0:T(8,128)(2,1)S(1)}, u32[]{:S(2)}, u32[]{:S(2)}) async-start(bf16[8,60,2048]{2,1,0:T(8,128)(2,1)} %reshape.371), calls=%async_computation.1 | async-start | bytes 4194304 | tf_op jit(solution)/shard_map/all_to_all | solution.py:183
  93.2 165.4 %all-gather.17.cloned.1.call-start = ((), (), s32[]{:S(2)}) async-start(), calls=%async_computation.8 | async-start | bytes 6291456 | tf_op jit(solution)/shard_map/all_gather | solution.py:181
  143.7 56.7 %copy-start.5 = (bf16[480,2048]{1,0:T(8,128)(2,1)S(1)}, bf16[480,2048]{1,0:T(8,128)(2,1)}, u32[]{:S(2)}) copy-start(bf16[480,2048]{1,0:T(8,128)(2,1)} %reshape.372) | copy-start | bytes 5898244
  258.6 3.1 copy-start.14
  258.6 3.2 copy-start.15
  264.5 4.8 %copy-start.13 = (f32[80,4]{0,1:T(4,128)S(1)}, f32[80,4]{0,1:T(4,128)}, u32[]{:S(2)}) copy-start(f32[80,4]{0,1:T(4,128)} %param.29) | copy-start | bytes 3844
  264.5 53.9 %all-to-all-start.1 = ((bf16[8,60,2048]{2,1,0:T(8,128)(2,1)}), bf16[8,60,2048]{2,1,0:T(8,128)(2,1)}, u32[]{:S(2)}, u32[]{:S(2)}) async-start(bf16[8,60,2048]{2,1,0:T(8,128)(2,1)} %reshape.373), calls=%async_computation.2 | async-start | bytes 4194304 | tf_op jit(solution)/shard_map/all_to_all | solution.py:187
  325.8 1.9 copy-start.4
Sparse Core Ops, SparseCore 0:
  10.4 26.7 all-gather.8
  38.9 22.9 all-gather.10
  68.5 15.5 reduce-scatter.1
  85.5 56.7 all-gather.14
  143.6 56.7 all-gather.12
  201.8 56.7 all-gather.16
where the time goes:
time: 336 us; the launch traced here: 335 us
  waiting for transfers between devices  239 us (71%)
  matrix products  33 us (10%)
  blocking collectives  16.3 us (5%)
  local copies, waits for them, and re-layouts  14.6 us (4%)
  between operations  13.9 us (4%)
  starting transfers between devices  9.75 us (3%)
  other arithmetic  8.39 us (2%)
    all_gather x1, waiting for transfers between devices, on_device(): lax.all_gather(down_w, 'tp', axis=0, tiled=True)  51.7 us
    all_gather x1, waiting for transfers between devices, on_device(): lax.all_gather(up_w, 'tp', axis=1, tiled=True)  50.3 us
    all_to_all x1, waiting for transfers between devices, on_device(): lax.all_to_all(result_rows.reshape(experts_all, capacity, model_width), '...  48.9 us
    all_to_all x1, waiting for transfers between devices, on_device(): lax.all_to_all(outgoing, 'sp', split_axis=0, concat_axis=0, tiled=True)  48.5 us
    all_gather x1, waiting for transfers between devices, on_device(): piece_values = lax.all_gather(values, 'sp', axis=0, tiled=True)  18.7 us
    all_gather x1, blocking collectives, on_device(): piece_pairs = lax.all_gather(key_pairs, 'sp', axis=0, tiled=True)  16.3 us
    reduce_scatter x1, waiting for transfers between devices, on_device(): lax.psum_scatter(jnp.dot(attended, own_rows, preferred_element_type=jnp.f...  12.7 us
    all_gather x1, waiting for transfers between devices, on_device(): piece_keys = lax.all_gather(key_plain, 'sp', axis=0, tiled=True)  7.27 us
  transfers between devices with their start and end apart: 8, of which 7 were waited for; matrix products, arithmetic and copies ran while one was open for 9% of the time, Pallas kernels for 0%

commit v1 on v0

--- a/solution.py
+++ b/solution.py
@@ -177,7 +177,7 @@
     group = lax.axis_size("tp")
     gate_full, up_full, down_full = (
         lax.all_gather(gate_w, "tp", axis=1, tiled=True),
-        lax.all_gather(up_w, "tp", axis=1, tiled=True),
+        jnp.concatenate(lax.all_gather(up_w, "tp"), axis=1),
         lax.all_gather(down_w, "tp", axis=0, tiled=True),
     )
     arrived = lax.all_to_all(outgoing, "sp", split_axis=0, concat_axis=0, tiled=True)

time: 336 us -> 336 us (level)
  waiting for transfers between devices: 239 us -> 232 us
  local copies, waits for them, and re-layouts: 14.6 us -> 20.9 us
    all_to_all x1, waiting for transfers between devices: 48.5 us -> 0.01 us  [on_device(): lax.all_to_all(outgoing, 'sp', split_axis=0, concat_axis=0, tiled=True)]
    all_gather x1, waiting for transfers between devices: 0.01 us -> 43.1 us  [on_device(): lax.all_gather(gate_w, 'tp', axis=1, tiled=True)]
    all_gather x0 -> x1, local copies, waits for them, and re-layouts: none -> 6.26 us  [on_device(): lax.all_gather(up_w, 'tp')]
  transfers between devices with their start and end apart: 8 -> 8, of which waited for: 7 -> 7; matrix products, arithmetic and copies ran while one was open for 9% -> 11% of each run, Pallas kernels for 0% -> 0%
where the time goes in v1:
time: 336 us; the launch traced here: 335 us
  waiting for transfers between devices  232 us (69%)
  matrix products  33.9 us (10%)
  local copies, waits for them, and re-layouts  20.9 us (6%)
  blocking collectives  16.3 us (5%)
  between operations  13.9 us (4%)
  starting transfers between devices  9.75 us (3%)
  other arithmetic  8.39 us (2%)
    all_gather x1, waiting for transfers between devices, on_device(): lax.all_gather(down_w, 'tp', axis=0, tiled=True)  51.7 us
    all_to_all x1, waiting for transfers between devices, on_device(): lax.all_to_all(result_rows.reshape(experts_all, capacity, model_width), '...  48.9 us
    all_gather x1, waiting for transfers between devices, on_device(): lax.all_gather(up_w, 'tp')  48.5 us
    all_gather x1, waiting for transfers between devices, on_device(): lax.all_gather(gate_w, 'tp', axis=1, tiled=True)  43.1 us
    all_gather x1, waiting for transfers between devices, on_device(): piece_values = lax.all_gather(values, 'sp', axis=0, tiled=True)  18.7 us
    all_gather x1, blocking collectives, on_device(): piece_pairs = lax.all_gather(key_pairs, 'sp', axis=0, tiled=True)  16.3 us
    reduce_scatter x1, waiting for transfers between devices, on_device(): lax.psum_scatter(jnp.dot(attended, own_rows, preferred_element_type=jnp.f...  12.7 us
    dot_general x1, matrix products, expert_active(): jnp.dot(rows, up_w, preferred_element_type=jnp.float32)  7.32 us
  transfers between devices with their start and end apart: 8, of which 7 were waited for; matrix products, arithmetic and copies ran while one was open for 11% of the time, Pallas kernels for 0%

profile of v1, /device:TPU:0, one launch (start us, length us, event | category | flops | bytes accessed | tf_op | source)
XLA Modules:
  0.0 335.5 jit_solution(4428656727196875114)
XLA Ops:
  8.4 1.9 convolution_convert_fusion.5
  10.3 2.1 convolution_convert_fusion.4
  13.1 16.3 %all_gather.19 = bf16[640,128]{1,0:T(8,128)(2,1)S(1)} all-gather(bf16[80,128]{1,0:T(8,128)(2,1)S(1)} %convert_element_type.125), channel_id=1, replica_groups=mesh['grp'=2,'sp'=8,'tp'=2] {'sp'}, dimensions={0}, use_global_device_ids=true | all-gather | bytes 184320 | tf_op jit(solution)/shard_map/all_gather | solution.py:112
  30.0 7.3 %all-gather.8.cloned.1.call-done = bf16[1280,512]{1,0:T(8,128)(2,1)} async-done(((bf16[160,512]{1,0:T(8,128)(2,1)}), bf16[1280,512]{1,0:T(8,128)(2,1)}) %all-gather.8.cloned.1.call-update) | async-done | bytes 1310736 | tf_op jit(solution)/shard_map/all_gather | solution.py:110
  43.1 18.7 %all-gather.10.cloned.1.call-done = bf16[1280,512]{1,0:T(8,128)(2,1)} async-done(((bf16[160,512]{1,0:T(8,128)(2,1)}), bf16[1280,512]{1,0:T(8,128)(2,1)}) %all-gather.10.cloned.1.call-update) | async-done | bytes 1310736 | tf_op jit(solution)/shard_map/all_gather | solution.py:111
  65.3 3.0 convolution_convert_fusion.3
  71.4 12.7 %reduce-scatter.2.cloned.1.call-done = bf16[80,2048]{1,0:T(8,128)(2,1)} async-done(((bf16[160,2048]{1,0:T(8,128)(2,1)}), bf16[80,2048]{1,0:T(8,128)(2,1)}) %reduce-scatter.2.cloned.1.call-update) | async-done | bytes 327696 | tf_op jit(solution)/shard_map/reduce_scatter | solution.py:147
  85.3 1.7 convolution_convert_fusion.2
  87.0 1.6 reshape.377
  88.6 4.6 %all-to-all-start = ((bf16[8,60,2048]{2,1,0:T(8,128)(2,1)}), bf16[8,60,2048]{2,1,0:T(8,128)(2,1)S(1)}, u32[]{:S(2)}, u32[]{:S(2)}) async-start(bf16[8,60,2048]{2,1,0:T(8,128)(2,1)} %reshape.377), calls=%async_computation.1 | async-start | bytes 4194304 | tf_op jit(solution)/shard_map/all_to_all | solution.py:183
  93.7 48.5 %all-gather.12.cloned.1.call-done = bf16[2,2048,512]{2,1,0:T(8,128)(2,1)} async-done(((bf16[1,2048,512]{2,1,0:T(8,128)(2,1)}), bf16[2,2048,512]{2,1,0:T(8,128)(2,1)}) %all-gather.12.cloned.1.call-update) | async-done | bytes 4194320 | tf_op jit(solution)/shard_map/all_gather | solution.py:180
  142.2 6.3 %copy.50 = bf16[2,2048,512]{1,2,0:T(8,128)(2,1)} copy(bf16[2,2048,512]{2,1,0:T(8,128)(2,1)} %all-gather.12.cloned.1.call-done) | data formatting | bytes 8388608 | tf_op jit(solution)/shard_map/all_gather | solution.py:180
  150.0 7.3 %fusion.82 = f32[480,1024]{1,0:T(8,128)} fusion(bf16[480,2048]{1,0:T(8,128)(2,1)} %reshape.378, bf16[2048,1024]{0,1:T(8,128)(2,1)} %bitcast.93), kind=kOutput, calls=%fused_computation.151 | convolution fusion | flops 2013265920 | bytes 8126464 | tf_op jit(solution)/shard_map/dot_general | solution.py:52
  157.3 43.1 %all-gather.14.cloned.1.call-done = bf16[1,2048,1024]{2,1,0:T(8,128)(2,1)} async-done(((bf16[1,2048,512]{2,1,0:T(8,128)(2,1)}), bf16[1,2048,1024]{2,1,0:T(8,128)(2,1)}) %all-gather.14.cloned.1.call-update) | async-done | bytes 4194320 | tf_op jit(solution)/shard_map/all_gather | solution.py:179
  200.4 6.4 %multiply_convert_fusion = bf16[480,1024]{1,0:T(8,128)(2,1)} fusion(f32[480,1024]{1,0:T(8,128)} %fusion.82, bf16[480,2048]{1,0:T(8,128)(2,1)S(1)} %copy-done.6, bf16[1,2048,1024]{2,1,0:T(8,128)(2,1)} %all-gather.14.cloned.1.call-done), kind=kOutput, calls=%fused_computation.24 | convolution fusion | flops 2018181120 | bytes 9109504 | tf_op jit(solution)/shard_map/dot_general | solution.py:51
  206.8 51.7 %all-gather.16.cloned.1.call-done = bf16[1,1024,2048]{2,1,0:T(8,128)(2,1)} async-done(((bf16[1,512,2048]{2,1,0:T(8,128)(2,1)}), bf16[1,1024,2048]{2,1,0:T(8,128)(2,1)}) %all-gather.16.cloned.1.call-update) | async-done | bytes 4194320 | tf_op jit(solution)/shard_map/all_gather | solution.py:181
  258.6 3.1 convolution_convert_fusion
  263.0 1.5 reshape.381
  264.5 4.7 %all-to-all-start.1 = ((bf16[8,60,2048]{2,1,0:T(8,128)(2,1)}), bf16[8,60,2048]{2,1,0:T(8,128)(2,1)}, u32[]{:S(2)}, u32[]{:S(2)}) async-start(bf16[8,60,2048]{2,1,0:T(8,128)(2,1)} %reshape.381), calls=%async_computation.2 | async-start | bytes 4194304 | tf_op jit(solution)/shard_map/all_to_all | solution.py:187
  269.5 48.9 %all-to-all-done.1 = bf16[8,60,2048]{2,1,0:T(8,128)(2,1)} async-done(((bf16[8,60,2048]{2,1,0:T(8,128)(2,1)}), bf16[8,60,2048]{2,1,0:T(8,128)(2,1)}, u32[]{:S(2)}, u32[]{:S(2)}) %all-to-all-start.1) | async-done | bytes 1966112 | tf_op jit(solution)/shard_map/all_to_all | solution.py:187
  318.4 1.7 reshape.382
  320.1 3.0 gather_fusion
  323.2 2.7 reshape.386
  325.9 1.9 multiply_reduce_fusion
  (108 shorter events, 20.8 us)
Async XLA Ops:
  6.5 1.9 copy-start
  6.5 6.0 %copy-start.11 = (bf16[160,64]{0,1:T(8,128)(2,1)S(1)}, bf16[160,64]{0,1:T(8,128)(2,1)}, u32[]{:S(2)}) copy-start(bf16[160,64]{0,1:T(8,128)(2,1)} %param.18) | copy-start | bytes 61444
  6.5 6.0 %copy-start.10 = (bf16[160,256]{1,0:T(8,128)(2,1)S(1)}, bf16[160,256]{1,0:T(8,128)(2,1)}, u32[]{:S(2)}) copy-start(bf16[160,256]{1,0:T(8,128)(2,1)} %param.16) | copy-start | bytes 245764
  6.5 23.0 %copy-start.9 = (bf16[160,512]{1,0:T(8,128)(2,1)S(1)}, bf16[160,512]{1,0:T(8,128)(2,1)}, u32[]{:S(2)}) copy-start(bf16[160,512]{1,0:T(8,128)(2,1)} %param.15) | copy-start | bytes 491524
  6.5 30.7 %all-gather.8.cloned.1.call-start = ((), (), s32[]{:S(2)}) async-start(), calls=%async_computation.3 | async-start | bytes 1474560 | tf_op jit(solution)/shard_map/all_gather | solution.py:110
  10.3 51.6 %all-gather.10.cloned.1.call-start = ((), (), s32[]{:S(2)}) async-start(), calls=%async_computation.4 | async-start | bytes 1474560 | tf_op jit(solution)/shard_map/all_gather | solution.py:111
  12.4 71.7 %reduce-scatter.2.cloned.1.call-start = ((), (), s32[]{:S(2)}) async-start(), calls=%async_computation.5 | async-start | bytes 983040 | tf_op jit(solution)/shard_map/reduce_scatter | solution.py:147
  37.2 1.8 copy-start.7
  61.8 2.8 copy-start.8
  61.8 3.1 copy-start.3
  68.3 1.2 copy-start.13
  68.3 2.9 copy-start.12
  68.4 15.7 %copy-start.4 = (bf16[80,2048]{1,0:T(8,128)(2,1)S(1)}, bf16[80,2048]{1,0:T(8,128)(2,1)}, u32[]{:S(2)}) copy-start(bf16[80,2048]{1,0:T(8,128)(2,1)} %param.22) | copy-start | bytes 983044
  68.4 73.9 %all-gather.12.cloned.1.call-start = ((), (), s32[]{:S(2)}) async-start(), calls=%async_computation.6 | async-start | bytes 6291456 | tf_op jit(solution)/shard_map/all_gather | solution.py:180
  68.9 131.4 %all-gather.14.cloned.1.call-start = ((), (), s32[]{:S(2)}) async-start(), calls=%async_computation.7 | async-start | bytes 6291456 | tf_op jit(solution)/shard_map/all_gather | solution.py:179
  88.6 59.9 %all-to-all-start = ((bf16[8,60,2048]{2,1,0:T(8,128)(2,1)}), bf16[8,60,2048]{2,1,0:T(8,128)(2,1)S(1)}, u32[]{:S(2)}, u32[]{:S(2)}) async-start(bf16[8,60,2048]{2,1,0:T(8,128)(2,1)} %reshape.377), calls=%async_computation.1 | async-start | bytes 4194304 | tf_op jit(solution)/shard_map/all_to_all | solution.py:183
  93.2 165.4 %all-gather.16.cloned.1.call-start = ((), (), s32[]{:S(2)}) async-start(), calls=%async_computation.8 | async-start | bytes 6291456 | tf_op jit(solution)/shard_map/all_gather | solution.py:181
  150.0 50.4 %copy-start.6 = (bf16[480,2048]{1,0:T(8,128)(2,1)S(1)}, bf16[480,2048]{1,0:T(8,128)(2,1)}, u32[]{:S(2)}) copy-start(bf16[480,2048]{1,0:T(8,128)(2,1)} %reshape.378) | copy-start | bytes 5898244
  258.6 3.1 copy-start.15
  258.6 3.2 copy-start.16
  264.5 4.8 %copy-start.14 = (f32[80,4]{0,1:T(4,128)S(1)}, f32[80,4]{0,1:T(4,128)}, u32[]{:S(2)}) copy-start(f32[80,4]{0,1:T(4,128)} %param.29) | copy-start | bytes 3844
  264.5 53.9 %all-to-all-start.1 = ((bf16[8,60,2048]{2,1,0:T(8,128)(2,1)}), bf16[8,60,2048]{2,1,0:T(8,128)(2,1)}, u32[]{:S(2)}, u32[]{:S(2)}) async-start(bf16[8,60,2048]{2,1,0:T(8,128)(2,1)} %reshape.381), calls=%async_computation.2 | async-start | bytes 4194304 | tf_op jit(solution)/shard_map/all_to_all | solution.py:187
  323.2 5.5 %copy-start.1 = (bf16[512,512]{1,0:T(8,128)(2,1)S(1)}, bf16[512,512]{1,0:T(8,128)(2,1)}, u32[]{:S(2)}) copy-start(bf16[512,512]{1,0:T(8,128)(2,1)} %param.20) | copy-start | bytes 1572868
  325.8 1.9 copy-start.5
  (1 other events, 0.9 us)
Sparse Core Ops, SparseCore 0:
  10.4 26.7 all-gather.7
  38.9 22.9 all-gather.9
  68.5 15.5 reduce-scatter.1
  85.5 56.7 all-gather.11
  143.6 56.7 all-gather.13
  201.8 56.7 all-gather.15
